TPU v7x, 32 devices: a whole 2x2x4 slice. The times are simulated.
32 devices in a mesh: grp: 2 (over y), fs: 4 (over z), tp: 4 (over x, core).
Axes of the slice: x: 2, y: 2, z: 4, core: 2. Of those that a mesh axis runs over, the one named last changes fastest.
Arguments:
- tokens: bfloat16 [8, 384, 2048], P(('grp', 'fs'), None, 'tp'), parts along dimension 0, may hold values from -24 to 24
- input_gain: float32 [2048], replicated, may hold values from 0.1 to 1.9
- query_weight: bfloat16 [2048, 1024], P('fs', 'tp'), may hold values from -0.125 to 0.125
- key_weight: bfloat16 [2048, 1024], P('fs', 'tp'), may hold values from -0.125 to 0.125
- value_weight: bfloat16 [2048, 1024], P('fs', 'tp'), may hold values from -0.125 to 0.125
- output_gate_matrix: bfloat16 [2048, 1024], P('fs', 'tp'), may hold values from -0.125 to 0.125
- forward_decay: float32 [16], P('tp'), may hold values from -1 to 9
- backward_decay: float32 [16], P('tp'), may hold values from -1 to 9
- merge_weight: bfloat16 [1024, 2048], P('tp', 'fs'), may hold values from -0.375 to 0.375
- middle_gain: float32 [2048], replicated, may hold values from 0.1 to 1.9
- gate_weight: bfloat16 [2048, 5120], P('fs', 'tp'), may hold values from -0.125 to 0.125
- up_weight: bfloat16 [2048, 5120], P('fs', 'tp'), may hold values from -0.125 to 0.125
- down_weight: bfloat16 [5120, 2048], P('tp', 'fs'), may hold values from -0.15625 to 0.15625
Outputs:
- layer_out: bfloat16 [8, 384, 2048], P(('grp', 'fs'), None, 'tp'), parts along dimension 0
There are 2 independent parts, one for each index of `grp`. A program takes and returns all parts, laid end to end along the dimension named above; an argument that names none is the same for every part. Nothing has to cross between parts.
All inputs are finite; a program needn't handle non-finite values.
Results may differ from a plain program's by a relative error of at most 0.019.
Values may be sent and summed in bfloat16 or wider, within the bound.
A program may use at most 64 MiB of HBM per device.

v0:
```python
import jax
import jax.numpy as jnp
from jax import lax
from jax.sharding import PartitionSpec as P

BLOCK = 128
norm_eps = 1e-06
group_eps = 1e-05
rope_base = 10000.0
highest_precision = lax.Precision.HIGHEST


def rms_scale(values, gain_vector):
    widened = values.astype(jnp.float32)
    scaled = widened * lax.rsqrt(jnp.mean(widened * widened, axis=-1, keepdims=True) + norm_eps)
    return (scaled * gain_vector).astype(jnp.bfloat16)


def apply_rotary_heads(values, length):
    half_dim = values.shape[-1] // 2
    inverse = rope_base ** (-jnp.arange(half_dim, dtype=jnp.float32) / half_dim)
    angles = jnp.arange(length, dtype=jnp.float32)[:, None] * inverse[None, :]
    cosine = jnp.cos(angles)[:, None, :]
    sine_part = jnp.sin(angles)[:, None, :]
    lower_half = values[..., :half_dim]
    upper_half = values[..., half_dim:]
    return jnp.concatenate(
        [
            lower_half * cosine - upper_half * sine_part,
            upper_half * cosine + lower_half * sine_part,
        ],
        axis=-1,
    )


def carry_states(key_blocks, value_blocks, weighting, log_rates, block_size, backward):
    block_terms = jnp.einsum(
        "sbmhd,sbmhe->bshde",
        key_blocks * weighting[None, None, :, :, None],
        value_blocks,
        precision=highest_precision,
    )
    factor = jnp.exp(log_rates * block_size)[None, :, None, None]

    def advance(running, addend):
        return (running * factor + addend, running)

    initial = jnp.zeros(block_terms.shape[1:], jnp.float32)
    return lax.scan(advance, initial, block_terms, reverse=backward)[1]


def retain_blocks(
    query_rows, key_rows, value_rows, gate_rows, forward_decay, backward_decay, seq_count, length
):
    head_count = forward_decay.shape[0]
    head_dim = query_rows.shape[1] // head_count
    block_size = BLOCK
    block_count = length // block_size

    def split_heads(rows_in):
        return rows_in.astype(jnp.float32).reshape(seq_count, length, head_count, head_dim)

    def blocked(tensor):
        return tensor.reshape(seq_count, block_count, block_size, head_count, head_dim)

    queries = blocked(apply_rotary_heads(split_heads(query_rows), length))
    key_heads = blocked(apply_rotary_heads(split_heads(key_rows), length) * head_dim ** (-0.5))
    valued = blocked(split_heads(value_rows))
    rate_ahead = jax.nn.log_sigmoid(forward_decay)
    rate_behind = jax.nn.log_sigmoid(backward_decay)
    position = jnp.arange(block_size, dtype=jnp.float32)
    offset = position[:, None] - position[None, :]
    inside = jnp.where(
        offset[None] >= 0,
        jnp.exp(rate_ahead[:, None, None] * jnp.maximum(offset, 0.0)[None]),
        jnp.exp(rate_behind[:, None, None] * jnp.maximum(-offset, 0.0)[None]),
    )
    attention_scores = (
        jnp.einsum("sbchd,sbmhd->sbhcm", queries, key_heads, precision=highest_precision)
        * inside[None, None]
    )
    result = jnp.einsum("sbhcm,sbmhd->sbchd", attention_scores, valued, precision=highest_precision)
    column = position[:, None]
    key_ahead = jnp.exp(rate_ahead[None, :] * (block_size - 1 - column))
    query_ahead = jnp.exp(rate_ahead[None, :] * (column + 1))
    key_behind = jnp.exp(rate_behind[None, :] * column)
    query_behind = jnp.exp(rate_behind[None, :] * (block_size - column))
    from_before = carry_states(key_heads, valued, key_ahead, rate_ahead, block_size, False)
    from_after = carry_states(key_heads, valued, key_behind, rate_behind, block_size, True)
    result = (
        result
        + jnp.einsum("sbchd,bshde->sbche", queries, from_before, precision=highest_precision)
        * query_ahead[None, None, :, :, None]
    )
    result = (
        result
        + jnp.einsum("sbchd,bshde->sbche", queries, from_after, precision=highest_precision)
        * query_behind[None, None, :, :, None]
    )
    result = result.reshape(seq_count, length, head_count, head_dim)
    center = jnp.mean(result, axis=-1, keepdims=True)
    spread = jnp.mean(jnp.square(result - center), axis=-1, keepdims=True)
    normalized = (result - center) * lax.rsqrt(spread + group_eps)
    gated = jax.nn.silu(split_heads(gate_rows)) * normalized
    return gated.reshape(seq_count * length, head_count * head_dim).astype(jnp.bfloat16)


def accumulate(pieces, source):
    return tuple(
        (
            jnp.dot(source, weight_piece, preferred_element_type=jnp.float32)
            for weight_piece in pieces
        )
    )


def on_device(
    tokens,
    input_gain,
    query_weight,
    key_weight,
    value_weight,
    output_gate_matrix,
    forward_decay,
    backward_decay,
    merge_weight,
    middle_gain,
    gate_weight,
    up_weight,
    down_weight,
):
    seq_count, length, part_width = tokens.shape
    row_count = seq_count * length
    gathered = lax.all_gather(tokens, "tp", axis=2, tiled=True)
    normed = rms_scale(gathered.reshape(row_count, gathered.shape[2]), input_gain)
    query_sum, key_sum, value_sum, gating_sum = accumulate(
        (
            lax.all_gather(query_weight, "fs", axis=0, tiled=True),
            lax.all_gather(key_weight, "fs", axis=0, tiled=True),
            lax.all_gather(value_weight, "fs", axis=0, tiled=True),
            lax.all_gather(output_gate_matrix, "fs", axis=0, tiled=True),
        ),
        normed,
    )
    mixed = retain_blocks(
        query_sum.astype(jnp.bfloat16),
        key_sum.astype(jnp.bfloat16),
        value_sum.astype(jnp.bfloat16),
        gating_sum.astype(jnp.bfloat16),
        forward_decay,
        backward_decay,
        seq_count,
        length,
    )
    merge_term = jnp.dot(
        mixed,
        lax.all_gather(merge_weight, "fs", axis=1, tiled=True),
        preferred_element_type=jnp.float32,
    )
    merged = lax.psum_scatter(
        merge_term.astype(jnp.bfloat16), "tp", scatter_dimension=1, tiled=True
    ).astype(jnp.float32)
    middle = (tokens.reshape(row_count, part_width).astype(jnp.float32) + merged).astype(
        jnp.bfloat16
    )
    gathered_mid = lax.all_gather(middle, "tp", axis=1, tiled=True)
    normed_mid = rms_scale(gathered_mid, middle_gain)
    gate_full, up_full = (
        lax.all_gather(gate_weight, "fs", axis=0, tiled=True),
        lax.all_gather(up_weight, "fs", axis=0, tiled=True),
    )
    gate_act = jnp.dot(normed_mid, gate_full, preferred_element_type=jnp.float32)
    up_act = jnp.dot(normed_mid, up_full, preferred_element_type=jnp.float32)
    hidden = (jax.nn.silu(gate_act) * up_act).astype(jnp.bfloat16)
    down_term = jnp.dot(
        hidden,
        lax.all_gather(down_weight, "fs", axis=1, tiled=True),
        preferred_element_type=jnp.float32,
    )
    summed = lax.psum_scatter(
        down_term.astype(jnp.bfloat16), "tp", scatter_dimension=1, tiled=True
    ).astype(jnp.float32)
    layer_out = (middle.astype(jnp.float32) + summed).astype(jnp.bfloat16)
    return layer_out.reshape(seq_count, length, part_width)


def solution(mesh):
    placed = (
        P(("grp", "fs"), None, "tp"),
        P(),
        P("fs", "tp"),
        P("fs", "tp"),
        P("fs", "tp"),
        P("fs", "tp"),
        P("tp"),
        P("tp"),
        P("tp", "fs"),
        P(),
        P("fs", "tp"),
        P("fs", "tp"),
        P("tp", "fs"),
    )
    return jax.shard_map(
        on_device,
        mesh=mesh,
        in_specs=placed,
        out_specs=P(("grp", "fs"), None, "tp"),
        check_vma=False,
    )
```

profile of v0, /device:TPU:0, one launch (start us, length us, event | category | flops | bytes accessed | tf_op | source)
XLA Modules:
  0.0 571.5 jit_solution(758774433648440747)
XLA Ops:
  6.5 0.7 all-gather.11.cloned.1.call-update
  13.1 18.2 %all-gather.11.cloned.1.call-done = bf16[1,384,2048]{2,1,0:T(8,128)(2,1)} async-done(((bf16[1,384,512]{2,1,0:T(8,128)(2,1)}), bf16[1,384,2048]{2,1,0:T(8,128)(2,1)}) %all-gather.11.cloned.1.call-update) | async-done | bytes 1572880 | tf_op jit(solution)/shard_map/all_gather | solution.py:134
  31.3 1.9 fusion.3
  33.2 27.7 %all-gather.17.cloned.1.call-done = bf16[2048,256]{1,0:T(8,128)(2,1)} async-done(((bf16[512,256]{1,0:T(8,128)(2,1)}), bf16[2048,256]{1,0:T(8,128)(2,1)}) %all-gather.17.cloned.1.call-update) | async-done | bytes 1048592 | tf_op jit(solution)/shard_map/all_gather | solution.py:138
  60.9 2.6 convolution_convert_fusion.3
  63.5 26.4 %all-gather.19.cloned.1.call-done = bf16[2048,256]{1,0:T(8,128)(2,1)} async-done(((bf16[512,256]{1,0:T(8,128)(2,1)}), bf16[2048,256]{1,0:T(8,128)(2,1)}) %all-gather.19.cloned.1.call-update) | async-done | bytes 1048592 | tf_op jit(solution)/shard_map/all_gather | solution.py:139
  89.8 2.1 convolution_convert_fusion.2
  92.0 0.9 multiply_subtract_fusion.1
  93.0 1.7 concatenate.22
  94.7 1.0 pad_maximum_fusion
  96.0 22.7 %all-gather.15.cloned.1.call-done = bf16[2048,256]{1,0:T(8,128)(2,1)} async-done(((bf16[512,256]{1,0:T(8,128)(2,1)}), bf16[2048,256]{1,0:T(8,128)(2,1)}) %all-gather.15.cloned.1.call-update) | async-done | bytes 1048592 | tf_op jit(solution)/shard_map/all_gather | solution.py:140
  118.6 2.6 convolution_convert_fusion.4
  121.2 1.2 reshape.432
  124.7 0.8 fusion.9
  125.5 0.8 fusion.10
  126.3 1.4 convolution_multiply_fusion.1
  127.8 0.9 fusion.43
  129.0 1.2 reshape.431
  130.8 16.7 %all-gather.13.cloned.1.call-done = bf16[2048,256]{1,0:T(8,128)(2,1)} async-done(((bf16[512,256]{1,0:T(8,128)(2,1)}), bf16[2048,256]{1,0:T(8,128)(2,1)}) %all-gather.13.cloned.1.call-update) | async-done | bytes 1048592 | tf_op jit(solution)/shard_map/all_gather | solution.py:141
  147.4 28.8 %all-gather.21.cloned.1.call-done = bf16[256,2048]{1,0:T(8,128)(2,1)} async-done(((bf16[256,512]{1,0:T(8,128)(2,1)}), bf16[256,2048]{1,0:T(8,128)(2,1)}) %all-gather.21.cloned.1.call-update) | async-done | bytes 1048592 | tf_op jit(solution)/shard_map/all_gather | solution.py:157
  176.3 4.7 convolution_convert_fusion.1
  181.1 27.5 %reduce-scatter.3.cloned.1.call-done = bf16[384,512]{1,0:T(8,128)(2,1)} async-done(((bf16[384,2048]{1,0:T(8,128)(2,1)}), bf16[384,512]{1,0:T(8,128)(2,1)}) %reduce-scatter.3.cloned.1.call-update) | async-done | bytes 393232 | tf_op jit(solution)/shard_map/reduce_scatter | solution.py:160
  208.5 1.8 fusion.12
  212.7 17.5 %all-gather.23.cloned.1.call-done = bf16[384,2048]{1,0:T(8,128)(2,1)} async-done(((bf16[384,512]{1,0:T(8,128)(2,1)}), bf16[384,2048]{1,0:T(8,128)(2,1)}) %all-gather.23.cloned.1.call-update) | async-done | bytes 1572880 | tf_op jit(solution)/shard_map/all_gather | solution.py:166
  230.2 1.8 fusion
  232.0 97.8 %all-gather.25.cloned.1.call-done = bf16[2048,1280]{1,0:T(8,128)(2,1)} async-done(((bf16[512,1280]{1,0:T(8,128)(2,1)}), bf16[2048,1280]{1,0:T(8,128)(2,1)}) %all-gather.25.cloned.1.call-update) | async-done | bytes 5242896 | tf_op jit(solution)/shard_map/all_gather | solution.py:169
  329.8 6.5 %fusion.15 = f32[384,1280]{1,0:T(8,128)} fusion(bf16[2048,1280]{1,0:T(8,128)(2,1)} %all-gather.25.cloned.1.call-done, bf16[384,2048]{1,0:T(8,128)(2,1)} %all-gather.23.cloned.1.call-done, f32[2048]{0:T(1024)S(1)} %copy-done.12, f32[384]{0:T(512)S(1)} %add_rsqrt_fusion), kind=kOutput, calls=%fused_computation.36 | convolution fusion | flops 2016411648 | bytes 8791552 | tf_op jit(solution)/shard_map/dot_general | solution.py:172
  336.4 91.3 %all-gather.27.cloned.1.call-done = bf16[2048,1280]{1,0:T(8,128)(2,1)} async-done(((bf16[512,1280]{1,0:T(8,128)(2,1)}), bf16[2048,1280]{1,0:T(8,128)(2,1)}) %all-gather.27.cloned.1.call-update) | async-done | bytes 5242896 | tf_op jit(solution)/shard_map/all_gather | solution.py:170
  427.7 98.0 %all-gather.29.cloned.1.call-done = bf16[1280,2048]{1,0:T(8,128)(2,1)} async-done(((bf16[1280,512]{1,0:T(8,128)(2,1)}), bf16[1280,2048]{1,0:T(8,128)(2,1)}) %all-gather.29.cloned.1.call-update) | async-done | bytes 5242896 | tf_op jit(solution)/shard_map/all_gather | solution.py:177
  525.6 10.7 %convolution_convert_fusion = bf16[384,2048]{1,0:T(8,128)(2,1)} fusion(bf16[1280,2048]{1,0:T(8,128)(2,1)} %all-gather.29.cloned.1.call-done, bf16[2048,1280]{1,0:T(8,128)(2,1)} %all-gather.27.cloned.1.call-done, f32[384,1280]{1,0:T(8,128)} %fusion.15, bf16[384,2048]{1,0:T(8,128)(2,1)S(1)} %copy-done.3, f32[2048]{0:T(1024)S(1)} %copy-done.12, ...), kind=kOutput, calls=%fused_computation.15 | convolution fusion | flops 4033413120 | bytes 15607296 | tf_op jit(solution)/shard_map/dot_general | solution.py:175
  536.3 26.5 %reduce-scatter.5.cloned.1.call-done = bf16[384,512]{1,0:T(8,128)(2,1)} async-done(((bf16[384,2048]{1,0:T(8,128)(2,1)}), bf16[384,512]{1,0:T(8,128)(2,1)}) %reduce-scatter.5.cloned.1.call-update) | async-done | bytes 393232 | tf_op jit(solution)/shard_map/reduce_scatter | solution.py:180
  562.8 1.8 fusion.17
  (97 shorter events, 12.1 us)
Async XLA Ops:
  6.5 54.3 %copy-start.10 = (f32[2048]{0:T(1024)S(1)}, f32[2048]{0:T(1024)}, u32[]{:S(2)}) copy-start(f32[2048]{0:T(1024)} %param.18) | copy-start | bytes 24580
  6.5 24.7 %all-gather.11.cloned.1.call-start = ((), (), s32[]{:S(2)}) async-start(), calls=%async_computation.2 | async-start | bytes 1966080 | tf_op jit(solution)/shard_map/all_gather | solution.py:134
  7.3 53.6 %all-gather.17.cloned.1.call-start = ((), (), s32[]{:S(2)}) async-start(), calls=%async_computation.5 | async-start | bytes 1310720 | tf_op jit(solution)/shard_map/all_gather | solution.py:138
  8.0 81.8 %all-gather.19.cloned.1.call-start = ((), (), s32[]{:S(2)}) async-start(), calls=%async_computation.6 | async-start | bytes 1310720 | tf_op jit(solution)/shard_map/all_gather | solution.py:139
  8.7 109.9 %all-gather.15.cloned.1.call-start = ((), (), s32[]{:S(2)}) async-start(), calls=%async_computation.4 | async-start | bytes 1310720 | tf_op jit(solution)/shard_map/all_gather | solution.py:140
  9.3 138.1 %all-gather.13.cloned.1.call-start = ((), (), s32[]{:S(2)}) async-start(), calls=%async_computation.3 | async-start | bytes 1310720 | tf_op jit(solution)/shard_map/all_gather | solution.py:141
  9.9 166.4 %all-gather.21.cloned.1.call-start = ((), (), s32[]{:S(2)}) async-start(), calls=%async_computation.7 | async-start | bytes 1310720 | tf_op jit(solution)/shard_map/all_gather | solution.py:157
  10.5 198.1 %reduce-scatter.3.cloned.1.call-start = ((), (), s32[]{:S(2)}) async-start(), calls=%async_computation.8 | async-start | bytes 1966080 | tf_op jit(solution)/shard_map/reduce_scatter | solution.py:160
  31.3 58.6 %copy-start.1 = (bf16[1,384,2048]{2,1,0:T(8,128)(2,1)S(1)}, bf16[1,384,2048]{2,1,0:T(8,128)(2,1)}, u32[]{:S(2)}) copy-start(bf16[1,384,2048]{2,1,0:T(8,128)(2,1)} %all-gather.11.cloned.1.call-done) | copy-start | bytes 4718596
  33.2 58.7 %copy-start.8 = (f32[384]{0:T(512)}, f32[384]{0:T(512)S(1)}, u32[]{:S(2)}) copy-start(f32[384]{0:T(512)S(1)} %add_rsqrt_fusion.1) | copy-start | bytes 4612
  95.9 26.7 %copy-start.5 = (f32[3,128,4,32]{1,0,3,2:T(4,128)S(1)}, f32[3,128,4,32]{1,0,3,2:T(4,128)}, u32[]{:S(2)}) copy-start(f32[3,128,4,32]{1,0,3,2:T(4,128)} %concatenate.22) | copy-start | bytes 589828
  95.9 26.7 %copy-start.6 = (f32[128,4]{0,1:T(4,128)S(1)}, f32[128,4]{0,1:T(4,128)}, u32[]{:S(2)}) copy-start(f32[128,4]{0,1:T(4,128)} %get-tuple-element.231) | copy-start | bytes 6148
  95.9 26.7 %copy-start.7 = (f32[128,4]{0,1:T(4,128)S(1)}, f32[128,4]{0,1:T(4,128)}, u32[]{:S(2)}) copy-start(f32[128,4]{0,1:T(4,128)} %get-tuple-element.229) | copy-start | bytes 6148
  127.8 48.5 %copy-start.2 = (bf16[1,384,2048]{2,1,0:T(8,128)(2,1)S(1)}, bf16[1,384,2048]{2,1,0:T(8,128)(2,1)}, u32[]{:S(2)}) copy-start(bf16[1,384,2048]{2,1,0:T(8,128)(2,1)} %all-gather.11.cloned.1.call-done) | copy-start | bytes 4718596
  127.8 48.5 %copy-start.9 = (f32[384]{0:T(512)S(1)}, f32[384]{0:T(512)}, u32[]{:S(2)}) copy-start(f32[384]{0:T(512)} %copy-done.8) | copy-start | bytes 4612
  127.8 48.5 %copy-start.11 = (f32[2048]{0:T(1024)S(1)}, f32[2048]{0:T(1024)}, u32[]{:S(2)}) copy-start(f32[2048]{0:T(1024)} %param.18) | copy-start | bytes 24580
  130.7 77.8 %copy-start.4 = (bf16[1,384,512]{2,1,0:T(8,128)(2,1)S(1)}, bf16[1,384,512]{2,1,0:T(8,128)(2,1)}, u32[]{:S(2)}) copy-start(bf16[1,384,512]{2,1,0:T(8,128)(2,1)} %param.17) | copy-start | bytes 1179652
  181.0 49.2 %all-gather.23.cloned.1.call-start = ((), (), s32[]{:S(2)}) async-start(), calls=%async_computation.9 | async-start | bytes 1966080 | tf_op jit(solution)/shard_map/all_gather | solution.py:166
  210.4 119.5 %copy-start.12 = (f32[2048]{0:T(1024)S(1)}, f32[2048]{0:T(1024)}, u32[]{:S(2)}) copy-start(f32[2048]{0:T(1024)} %param.26) | copy-start | bytes 24580
  210.4 119.4 %all-gather.25.cloned.1.call-start = ((), (), s32[]{:S(2)}) async-start(), calls=%async_computation.10 | async-start | bytes 6553600 | tf_op jit(solution)/shard_map/all_gather | solution.py:169
  211.1 216.5 %all-gather.27.cloned.1.call-start = ((), (), s32[]{:S(2)}) async-start(), calls=%async_computation.11 | async-start | bytes 6553600 | tf_op jit(solution)/shard_map/all_gather | solution.py:170
  211.7 313.9 %all-gather.29.cloned.1.call-start = ((), (), s32[]{:S(2)}) async-start(), calls=%async_computation.12 | async-start | bytes 6553600 | tf_op jit(solution)/shard_map/all_gather | solution.py:177
  212.5 350.4 %reduce-scatter.5.cloned.1.call-start = ((), (), s32[]{:S(2)}) async-start(), calls=%async_computation.13 | async-start | bytes 1966080 | tf_op jit(solution)/shard_map/reduce_scatter | solution.py:180
  232.0 293.6 %copy-start.3 = (bf16[384,2048]{1,0:T(8,128)(2,1)S(1)}, bf16[384,2048]{1,0:T(8,128)(2,1)}, u32[]{:S(2)}) copy-start(bf16[384,2048]{1,0:T(8,128)(2,1)} %all-gather.23.cloned.1.call-done) | copy-start | bytes 4718596
  336.4 226.4 %copy-start = (bf16[384,512]{1,0:T(8,128)(2,1)S(1)}, bf16[384,512]{1,0:T(8,128)(2,1)}, u32[]{:S(2)}) copy-start(bf16[384,512]{1,0:T(8,128)(2,1)} %fusion.12) | copy-start | bytes 1179652
Sparse Core Ops, SparseCore 0:
  8.9 22.3 all-gather.10
  32.8 27.9 all-gather.16
  62.4 27.3 all-gather.18
  91.3 27.3 all-gather.14
  120.1 27.3 all-gather.12
  148.9 27.3 all-gather.20
  181.1 27.3 reduce-scatter.2
  210.5 19.6 all-gather.22
  231.8 98.0 all-gather.24
  331.3 96.3 all-gather.26
  429.2 96.3 all-gather.28
  536.5 26.3 reduce-scatter.4
where the time goes:
time: 572 us; the launch traced here: 571 us
  waiting for transfers between devices  505 us (88%)
  matrix products  33.9 us (6%)
  between operations  13.9 us (2%)
  other arithmetic  12.9 us (2%)
    all_gather x1, waiting for transfers between devices, on_device(): lax.all_gather(down_weight, 'fs', axis=1, tiled=True)  98 us
    all_gather x1, waiting for transfers between devices, on_device(): lax.all_gather(gate_weight, 'fs', axis=0, tiled=True)  97.8 us
    all_gather x1, waiting for transfers between devices, on_device(): lax.all_gather(up_weight, 'fs', axis=0, tiled=True)  91.3 us
    all_gather x1, waiting for transfers between devices, on_device(): lax.all_gather(merge_weight, 'fs', axis=1, tiled=True)  28.8 us
    all_gather x1, waiting for transfers between devices, on_device(): lax.all_gather(query_weight, 'fs', axis=0, tiled=True)  27.7 us
    reduce_scatter x1, waiting for transfers between devices, on_device(): lax.psum_scatter(merge_term.astype(jnp.bfloat16), 'tp', scatter_dimension...  27.5 us
    reduce_scatter x1, waiting for transfers between devices, on_device(): lax.psum_scatter(down_term.astype(jnp.bfloat16), 'tp', scatter_dimension=...  26.5 us
    all_gather x1, waiting for transfers between devices, on_device(): lax.all_gather(key_weight, 'fs', axis=0, tiled=True)  26.4 us
  transfers between devices with their start and end apart: 12, of which 12 were waited for; matrix products, arithmetic and copies ran while one was open for 6% of the time, Pallas kernels for 0%

commit v1 on v0

--- a/solution.py
+++ b/solution.py
@@ -8,6 +8,19 @@
 group_eps = 1e-05
 rope_base = 10000.0
 highest_precision = lax.Precision.HIGHEST
+
+
+def ring_gather(array, axis, dim):
+    ways = lax.axis_size(axis)
+    up = [(d, (d + 1) % ways) for d in range(ways)]
+    down = [(d, (d - 1) % ways) for d in range(ways)]
+    earlier, later = ([array], [array])
+    for _ in range(ways // 2):
+        earlier.append(lax.ppermute(earlier[-1], axis, up))
+    for _ in range((ways - 1) // 2):
+        later.append(lax.ppermute(later[-1], axis, down))
+    line = jnp.concatenate([*earlier[::-1], *later[1:]], axis=dim)
+    return jnp.roll(line, (lax.axis_index(axis) - ways // 2) * array.shape[dim], axis=dim)
 
 
 def rms_scale(values, gain_vector):
@@ -173,9 +186,7 @@
     up_act = jnp.dot(normed_mid, up_full, preferred_element_type=jnp.float32)
     hidden = (jax.nn.silu(gate_act) * up_act).astype(jnp.bfloat16)
     down_term = jnp.dot(
-        hidden,
-        lax.all_gather(down_weight, "fs", axis=1, tiled=True),
-        preferred_element_type=jnp.float32,
+        hidden, ring_gather(down_weight, "fs", 1), preferred_element_type=jnp.float32
     )
     summed = lax.psum_scatter(
         down_term.astype(jnp.bfloat16), "tp", scatter_dimension=1, tiled=True

time: 572 us -> 529 us (0.925)
  waiting for transfers between devices: 505 us -> 449 us
  local copies, waits for them, and re-layouts: 5.47 us -> 17.1 us
    ppermute x0 -> x3, waiting for transfers between devices: none -> 138 us  [the longest x2 88.6 us: ring_gather(): earlier.append(lax.ppermute(earlier[-1], axis, up))]
    all_gather x1 -> x0, waiting for transfers between devices: 98 us -> none  [on_device(): lax.all_gather(down_weight, 'fs', axis=1, tiled=True)]
    all_gather x1, waiting for transfers between devices: 97.8 us -> 13.9 us  [on_device(): lax.all_gather(gate_weight, 'fs', axis=0, tiled=True)]
    all_gather x1, waiting for transfers between devices: 17.5 us -> 0.01 us  [on_device(): gathered_mid = lax.all_gather(middle, 'tp', axis=1, tiled=True)]
    unnamed x27 -> x24, local copies, waits for them, and re-layouts: 0.1 us -> 12.6 us
    all_gather x1, waiting for transfers between devices: 16.7 us -> 28.8 us  [on_device(): lax.all_gather(output_gate_matrix, 'fs', axis=0, tiled=True)]
    all_gather x1, waiting for transfers between devices: 28.8 us -> 18.8 us  [on_device(): lax.all_gather(merge_weight, 'fs', axis=1, tiled=True)]
  transfers between devices with their start and end apart: 12 -> 14, of which waited for: 12 -> 13; matrix products, arithmetic and copies ran while one was open for 6% -> 8% of each run, Pallas kernels for 0% -> 0%
where the time goes in v1:
time: 529 us
  waiting for transfers between devices  449 us (85%)
  matrix products  33.1 us (6%)
  local copies, waits for them, and re-layouts  17.1 us (3%)
  between operations  13.6 us (3%)
  other arithmetic  9.76 us (2%)
  starting transfers between devices  5.77 us (1%)
    all_gather x1, waiting for transfers between devices, on_device(): lax.all_gather(up_weight, 'fs', axis=0, tiled=True)  91.3 us
    ppermute x2, waiting for transfers between devices, ring_gather(): earlier.append(lax.ppermute(earlier[-1], axis, up))  88.6 us
    ppermute x1, waiting for transfers between devices, ring_gather(): later.append(lax.ppermute(later[-1], axis, down))  49.1 us
    all_gather x1, waiting for transfers between devices, on_device(): lax.all_gather(output_gate_matrix, 'fs', axis=0, tiled=True)  28.8 us
    all_gather x1, waiting for transfers between devices, on_device(): lax.all_gather(value_weight, 'fs', axis=0, tiled=True)  27.8 us
    reduce_scatter x1, waiting for transfers between devices, on_device(): lax.psum_scatter(merge_term.astype(jnp.bfloat16), 'tp', scatter_dimension...  27.5 us
    all_gather x1, waiting for transfers between devices, on_device(): lax.all_gather(key_weight, 'fs', axis=0, tiled=True)  26.7 us
    reduce_scatter x1, waiting for transfers between devices, on_device(): lax.psum_scatter(down_term.astype(jnp.bfloat16), 'tp', scatter_dimension=...  26.5 us
  transfers between devices with their start and end apart: 14, of which 13 were waited for; matrix products, arithmetic and copies ran while one was open for 8% of the time, Pallas kernels for 0%

profile of v1, /device:TPU:0, one launch (start us, length us, event | category | flops | bytes accessed | tf_op | source)
XLA Modules:
  0.0 528.9 jit_solution(12681799811731377722)
XLA Ops:
  11.9 19.3 %all-gather.10.cloned.1.call-done = bf16[1,384,2048]{2,1,0:T(8,128)(2,1)} async-done(((bf16[1,384,512]{2,1,0:T(8,128)(2,1)}), bf16[1,384,2048]{2,1,0:T(8,128)(2,1)}) %all-gather.10.cloned.1.call-update) | async-done | bytes 1572880 | tf_op jit(solution)/shard_map/all_gather | solution.py:147
  31.3 1.8 fusion.5
  33.1 27.8 %all-gather.14.cloned.1.call-done = bf16[2048,256]{1,0:T(8,128)(2,1)} async-done(((bf16[512,256]{1,0:T(8,128)(2,1)}), bf16[2048,256]{1,0:T(8,128)(2,1)}) %all-gather.14.cloned.1.call-update) | async-done | bytes 1048592 | tf_op jit(solution)/shard_map/all_gather | solution.py:153
  60.9 2.3 convolution_convert_fusion.3
  63.6 26.2 %all-gather.16.cloned.1.call-done = bf16[2048,256]{1,0:T(8,128)(2,1)} async-done(((bf16[512,256]{1,0:T(8,128)(2,1)}), bf16[2048,256]{1,0:T(8,128)(2,1)}) %all-gather.16.cloned.1.call-update) | async-done | bytes 1048592 | tf_op jit(solution)/shard_map/all_gather | solution.py:151
  89.8 2.1 convolution_convert_fusion.2
  92.0 26.7 %all-gather.18.cloned.1.call-done = bf16[2048,256]{1,0:T(8,128)(2,1)} async-done(((bf16[512,256]{1,0:T(8,128)(2,1)}), bf16[2048,256]{1,0:T(8,128)(2,1)}) %all-gather.18.cloned.1.call-update) | async-done | bytes 1048592 | tf_op jit(solution)/shard_map/all_gather | solution.py:152
  118.6 2.1 convolution_convert_fusion.1
  125.1 1.4 convolution_multiply_fusion.1
  128.7 18.8 %all-gather.20.cloned.1.call-done = bf16[256,2048]{1,0:T(8,128)(2,1)} async-done(((bf16[256,512]{1,0:T(8,128)(2,1)}), bf16[256,2048]{1,0:T(8,128)(2,1)}) %all-gather.20.cloned.1.call-update) | async-done | bytes 1048592 | tf_op jit(solution)/shard_map/all_gather | solution.py:170
  147.5 28.8 %all-gather.12.cloned.1.call-done = bf16[2048,256]{1,0:T(8,128)(2,1)} async-done(((bf16[512,256]{1,0:T(8,128)(2,1)}), bf16[2048,256]{1,0:T(8,128)(2,1)}) %all-gather.12.cloned.1.call-update) | async-done | bytes 1048592 | tf_op jit(solution)/shard_map/all_gather | solution.py:154
  176.3 4.6 convolution_convert_fusion
  180.9 27.5 %reduce-scatter.3.cloned.1.call-done = bf16[384,512]{1,0:T(8,128)(2,1)} async-done(((bf16[384,2048]{1,0:T(8,128)(2,1)}), bf16[384,512]{1,0:T(8,128)(2,1)}) %reduce-scatter.3.cloned.1.call-update) | async-done | bytes 393232 | tf_op jit(solution)/shard_map/reduce_scatter | solution.py:173
  208.4 1.8 fusion.18
  211.7 1.6 collective-permute-start
  213.2 30.8 %collective-permute-done = bf16[1280,512]{1,0:T(8,128)(2,1)S(1)} collective-permute-done((bf16[1280,512]{1,0:T(8,128)(2,1)S(1)}, bf16[1280,512]{1,0:T(8,128)(2,1)S(1)}, u32[]{:S(2)}, u32[]{:S(2)}) %collective-permute-start) | collective-permute-done | bytes 1310752 | tf_op jit(solution)/shard_map/ppermute | solution.py:19
  244.1 3.7 collective-permute-start.2
  247.8 57.8 %collective-permute-done.1 = bf16[1280,512]{1,0:T(8,128)(2,1)} collective-permute-done((bf16[1280,512]{1,0:T(8,128)(2,1)S(1)}, bf16[1280,512]{1,0:T(8,128)(2,1)}, u32[]{:S(2)}, u32[]{:S(2)}) %collective-permute-start.1) | collective-permute-done | bytes 1310752 | tf_op jit(solution)/shard_map/ppermute | solution.py:19
  305.6 2.5 constant_dynamic-update-slice_fusion.9
  309.4 1.3 constant_dynamic-update-slice_fusion.7
  310.6 49.1 %collective-permute-done.2 = bf16[1280,512]{1,0:T(8,128)(2,1)} collective-permute-done((bf16[1280,512]{1,0:T(8,128)(2,1)S(1)}, bf16[1280,512]{1,0:T(8,128)(2,1)}, u32[]{:S(2)}, u32[]{:S(2)}) %collective-permute-start.2) | collective-permute-done | bytes 1310752 | tf_op jit(solution)/shard_map/ppermute | solution.py:21
  359.7 2.6 constant_dynamic-update-slice_fusion.6
  362.3 2.6 constant_dynamic-update-slice_fusion.5
  364.9 1.3 constant_dynamic-update-slice_fusion.4
  367.3 2.5 constant_dynamic-update-slice_fusion.2
  369.8 1.8 fusion.2
  371.6 13.9 %all-gather.24.cloned.1.call-done = bf16[2048,1280]{1,0:T(8,128)(2,1)} async-done(((bf16[512,1280]{1,0:T(8,128)(2,1)}), bf16[2048,1280]{1,0:T(8,128)(2,1)}) %all-gather.24.cloned.1.call-update) | async-done | bytes 5242896 | tf_op jit(solution)/shard_map/all_gather | solution.py:182
  385.5 6.5 %fusion.21 = f32[384,1280]{1,0:T(8,128)} fusion(bf16[2048,1280]{1,0:T(8,128)(2,1)} %all-gather.24.cloned.1.call-done, bf16[384,2048]{1,0:T(8,128)(2,1)} %all-gather.22.cloned.1.call-done, f32[2048]{0:T(1024)S(1)} %copy-done.7, f32[384]{0:T(512)S(1)} %add_rsqrt_fusion), kind=kOutput, calls=%fused_computation.39 | convolution fusion | flops 2016411648 | bytes 8791552 | tf_op jit(solution)/shard_map/dot_general | solution.py:185
  392.1 91.3 %all-gather.26.cloned.1.call-done = bf16[2048,1280]{1,0:T(8,128)(2,1)} async-done(((bf16[512,1280]{1,0:T(8,128)(2,1)}), bf16[2048,1280]{1,0:T(8,128)(2,1)}) %all-gather.26.cloned.1.call-update) | async-done | bytes 5242896 | tf_op jit(solution)/shard_map/all_gather | solution.py:183
  483.4 10.7 %fusion.9 = bf16[384,2048]{1,0:T(8,128)(2,1)} fusion(bf16[1280,4096]{1,0:T(8,128)(2,1)} %constant_dynamic-update-slice_fusion.2, s32[]{:T(128)S(6)} %select_n.33, bf16[2048,1280]{1,0:T(8,128)(2,1)} %all-gather.26.cloned.1.call-done, f32[384,1280]{1,0:T(8,128)} %fusion.21, bf16[384,2048]{1,0:T(8,128)(2,1)S(1)} %copy-done.4, f32[2048]{0:T(1024)S(1)} %copy-done.7, ...), kind=kOutput, calls=%fused_computation.18 | convolution fusion | flops 4033413120 | bytes 15607300 | tf_op jit(solution)/shard_map/dot_general | solution.py:188
  494.1 26.5 %reduce-scatter.5.cloned.1.call-done = bf16[384,512]{1,0:T(8,128)(2,1)} async-done(((bf16[384,2048]{1,0:T(8,128)(2,1)}), bf16[384,512]{1,0:T(8,128)(2,1)}) %reduce-scatter.5.cloned.1.call-update) | async-done | bytes 393232 | tf_op jit(solution)/shard_map/reduce_scatter | solution.py:191
  520.6 1.8 fusion.23
  (98 shorter events, 16.6 us)
Async XLA Ops:
  6.5 54.3 %copy-start.6 = (f32[2048]{0:T(1024)S(1)}, f32[2048]{0:T(1024)}, u32[]{:S(2)}) copy-start(f32[2048]{0:T(1024)} %param.18) | copy-start | bytes 24580
  6.5 24.7 %all-gather.10.cloned.1.call-start = ((), (), s32[]{:S(2)}) async-start(), calls=%async_computation.2 | async-start | bytes 1966080 | tf_op jit(solution)/shard_map/all_gather | solution.py:147
  7.3 53.6 %all-gather.14.cloned.1.call-start = ((), (), s32[]{:S(2)}) async-start(), calls=%async_computation.4 | async-start | bytes 1310720 | tf_op jit(solution)/shard_map/all_gather | solution.py:153
  8.0 81.8 %all-gather.16.cloned.1.call-start = ((), (), s32[]{:S(2)}) async-start(), calls=%async_computation.5 | async-start | bytes 1310720 | tf_op jit(solution)/shard_map/all_gather | solution.py:151
  8.7 109.9 %all-gather.18.cloned.1.call-start = ((), (), s32[]{:S(2)}) async-start(), calls=%async_computation.6 | async-start | bytes 1310720 | tf_op jit(solution)/shard_map/all_gather | solution.py:152
  9.3 138.1 %all-gather.20.cloned.1.call-start = ((), (), s32[]{:S(2)}) async-start(), calls=%async_computation.7 | async-start | bytes 1310720 | tf_op jit(solution)/shard_map/all_gather | solution.py:170
  9.9 166.4 %all-gather.12.cloned.1.call-start = ((), (), s32[]{:S(2)}) async-start(), calls=%async_computation.3 | async-start | bytes 1310720 | tf_op jit(solution)/shard_map/all_gather | solution.py:154
  10.5 197.9 %reduce-scatter.3.cloned.1.call-start = ((), (), s32[]{:S(2)}) async-start(), calls=%async_computation.8 | async-start | bytes 1966080 | tf_op jit(solution)/shard_map/reduce_scatter | solution.py:173
  33.1 56.8 %copy-start.2 = (bf16[1,384,2048]{2,1,0:T(8,128)(2,1)S(1)}, bf16[1,384,2048]{2,1,0:T(8,128)(2,1)}, u32[]{:S(2)}) copy-start(bf16[1,384,2048]{2,1,0:T(8,128)(2,1)} %all-gather.10.cloned.1.call-done) | copy-start | bytes 4718596
  126.5 49.8 %copy-start.3 = (bf16[1,384,2048]{2,1,0:T(8,128)(2,1)S(1)}, bf16[1,384,2048]{2,1,0:T(8,128)(2,1)}, u32[]{:S(2)}) copy-start(bf16[1,384,2048]{2,1,0:T(8,128)(2,1)} %all-gather.10.cloned.1.call-done) | copy-start | bytes 4718596
  128.7 79.7 %copy-start.5 = (bf16[1,384,512]{2,1,0:T(8,128)(2,1)S(1)}, bf16[1,384,512]{2,1,0:T(8,128)(2,1)}, u32[]{:S(2)}) copy-start(bf16[1,384,512]{2,1,0:T(8,128)(2,1)} %param.17) | copy-start | bytes 1179652
  180.9 30.8 %copy-start = (bf16[1280,512]{1,0:T(8,128)(2,1)S(1)}, bf16[1280,512]{1,0:T(8,128)(2,1)}, u32[]{:S(2)}) copy-start(bf16[1280,512]{1,0:T(8,128)(2,1)} %param.29) | copy-start | bytes 3932164
  180.9 188.9 %all-gather.22.cloned.1.call-start = ((), (), s32[]{:S(2)}) async-start(), calls=%async_computation.9 | async-start | bytes 1966080 | tf_op jit(solution)/shard_map/all_gather | solution.py:179
  210.3 175.2 %all-gather.24.cloned.1.call-start = ((), (), s32[]{:S(2)}) async-start(), calls=%async_computation.10 | async-start | bytes 6553600 | tf_op jit(solution)/shard_map/all_gather | solution.py:182
  211.0 272.4 %all-gather.26.cloned.1.call-start = ((), (), s32[]{:S(2)}) async-start(), calls=%async_computation.11 | async-start | bytes 6553600 | tf_op jit(solution)/shard_map/all_gather | solution.py:183
  211.6 308.9 %reduce-scatter.5.cloned.1.call-start = ((), (), s32[]{:S(2)}) async-start(), calls=%async_computation.12 | async-start | bytes 1966080 | tf_op jit(solution)/shard_map/reduce_scatter | solution.py:191
  211.7 32.3 %collective-permute-start = (bf16[1280,512]{1,0:T(8,128)(2,1)S(1)}, bf16[1280,512]{1,0:T(8,128)(2,1)S(1)}, u32[]{:S(2)}, u32[]{:S(2)}) collective-permute-start(bf16[1280,512]{1,0:T(8,128)(2,1)S(1)} %copy-done), channel_id=1, source_target_pairs={{0,4},{4,8},{8,12},{12,0},{1,5},{5,9},{9,13},{13,1},{2,6},{6,10},{... | collective-permute-start | bytes 3932168 | tf_op jit(solution)/shard_map/ppermute | solution.py:19
  244.0 61.6 %collective-permute-start.1 = (bf16[1280,512]{1,0:T(8,128)(2,1)S(1)}, bf16[1280,512]{1,0:T(8,128)(2,1)}, u32[]{:S(2)}, u32[]{:S(2)}) collective-permute-start(bf16[1280,512]{1,0:T(8,128)(2,1)S(1)} %collective-permute-done), channel_id=1, source_target_pairs={{0,4},{4,8},{8,12},{12,0},{1,5},{5,9},{9,13},{13,1},{2,6},{6,10},{... | collective-permute-start | bytes 3932168 | tf_op jit(solution)/shard_map/ppermute | solution.py:19
  244.1 115.6 %collective-permute-start.2 = (bf16[1280,512]{1,0:T(8,128)(2,1)S(1)}, bf16[1280,512]{1,0:T(8,128)(2,1)}, u32[]{:S(2)}, u32[]{:S(2)}) collective-permute-start(bf16[1280,512]{1,0:T(8,128)(2,1)S(1)} %copy-done), channel_id=1, source_target_pairs={{0,12},{4,0},{8,4},{12,8},{1,13},{5,1},{9,5},{13,9},{2,14},{6,2},{... | collective-permute-start | bytes 3932168 | tf_op jit(solution)/shard_map/ppermute | solution.py:21
  366.1 19.4 %copy-start.7 = (f32[2048]{0:T(1024)S(1)}, f32[2048]{0:T(1024)}, u32[]{:S(2)}) copy-start(f32[2048]{0:T(1024)} %param.26) | copy-start | bytes 24580
  371.6 111.8 %copy-start.4 = (bf16[384,2048]{1,0:T(8,128)(2,1)S(1)}, bf16[384,2048]{1,0:T(8,128)(2,1)}, u32[]{:S(2)}) copy-start(bf16[384,2048]{1,0:T(8,128)(2,1)} %all-gather.22.cloned.1.call-done) | copy-start | bytes 4718596
  392.1 128.5 %copy-start.1 = (bf16[384,512]{1,0:T(8,128)(2,1)S(1)}, bf16[384,512]{1,0:T(8,128)(2,1)}, u32[]{:S(2)}) copy-start(bf16[384,512]{1,0:T(8,128)(2,1)} %fusion.18) | copy-start | bytes 1179652
Sparse Core Ops, SparseCore 0:
  8.9 22.3 all-gather.9
  32.8 27.9 all-gather.13
  62.4 27.3 all-gather.15
  91.3 27.3 all-gather.17
  120.1 27.3 all-gather.19
  148.9 27.3 all-gather.11
  181.0 27.3 reduce-scatter.2
  210.4 19.6 all-gather.21
  231.7 153.8 all-gather.23
  386.9 96.3 all-gather.25
  494.2 26.3 reduce-scatter.4
